TPU v7x, 512 devices: a whole 4x8x8 slice. The times are simulated.
512 devices in a mesh: sp: 128 (over z, y, core), tp: 4 (over x).
Axes of the slice: x: 4, y: 8, z: 8, core: 2. Of those that a mesh axis runs over, the one named last changes fastest.
Arguments:
- tokens: bfloat16 [16384, 2048], P(('sp', 'tp')), may hold values from -6 to 6
- norm_gain: float32 [2048], replicated, may hold values from 0.1 to 1.9
- w_filter_b: bfloat16 [2048, 1024], P('sp', 'tp'), may hold values from -0.125 to 0.125
- w_filter_c: bfloat16 [2048, 1024], P('sp', 'tp'), may hold values from -0.125 to 0.125
- w_filter_v: bfloat16 [2048, 1024], P('sp', 'tp'), may hold values from -0.125 to 0.125
- filter_taps: float32 [3, 1024], P(None, 'tp'), may hold values from -3.5 to 3.5
- w_query: bfloat16 [2048, 1024], P('sp', 'tp'), may hold values from -0.125 to 0.125
- retention_gate_matrix: bfloat16 [2048, 1024], P('sp', 'tp'), may hold values from -0.125 to 0.125
- w_input: bfloat16 [2048, 1024], P('sp', 'tp'), may hold values from -0.125 to 0.125
- forget_gap: float32 [1024], P('tp'), may hold values from 0 to 0.12
- additive_fade_log: float32 [16384, 1024], P('sp', 'tp'), may hold values from -1.1 to 0
- head_gain: float32 [128], replicated, may hold values from 0.1 to 1.9
- initial_state: float32 [8, 128, 128], P('tp'), may hold values from -0.013671875 to 0.013671875
- w_out_filter: bfloat16 [1024, 2048], P('tp'), may hold values from -0.125 to 0.125
- w_out_rec: bfloat16 [1024, 2048], P('tp'), may hold values from -0.125 to 0.125
Outputs:
- mixed: bfloat16 [16384, 2048], P(('sp', 'tp'))
All inputs are finite; a program needn't handle non-finite values.
Results may differ from a plain program's by a relative error of at most 0.03.
Values may be sent and summed in bfloat16 or wider, within the bound.
No kernel may reach another device: no remote copies, remote signals or barrier semaphores. Data moves between devices by JAX's collectives and lax.ppermute only.
A program may use at most 64 MiB of HBM per device.

v0:
```python
import jax
import jax.numpy as jnp
import numpy as np
from jax import lax
from jax.sharding import Mesh
from jax.sharding import PartitionSpec as P

HEAD_DIM = 128
SPAN = 64
TAPS = 3
HALO = 16
SP = ("sp_0", "sp_1", "sp_2")
SP_TP = ("sp_0", "sp_1", "sp_2", "tp")
epsilon = 1e-06
f32 = jnp.float32
bf16 = jnp.bfloat16


def exchanged(blocks, axis):
    return lax.all_to_all(blocks, axis, split_axis=0, concat_axis=0, tiled=True)


def sent_to_all(x, axis):
    return exchanged(jnp.broadcast_to(x, (lax.axis_size(axis), *x.shape)), axis)


def swapped(x, axis):
    return lax.ppermute(x, axis, [(0, 1), (1, 0)])


def shifted(block, axis):
    size = lax.axis_size(axis)
    return lax.ppermute(block, axis, [(i, i + 1) for i in range(size - 1)])


def running_sum(x):
    causal = jnp.tril(jnp.ones((x.shape[0], x.shape[0]), f32))
    return jnp.dot(causal, x, precision=lax.Precision.HIGHEST)


def rates(forget_logit, forget_gap, fade):
    key_rate = forget_gap * jax.nn.sigmoid(-forget_logit.astype(f32))
    return (key_rate, jnp.log1p(-key_rate) + fade)


def silu(v):
    return jax.nn.silu(v.astype(f32))


def state_of(key_rate, log_decay, value_in):
    running = running_sum(log_decay)
    remainder = (key_rate * jnp.exp(running[-1:] - running)).astype(bf16)
    state = jnp.einsum("tv,tk->vk", value_in.astype(bf16), remainder, preferred_element_type=f32)
    return (running[-1], state)


def pack(decay, state):
    high = lax.reduce_precision(decay, 8, 7)
    rest = decay - high
    low = lax.reduce_precision(rest, 8, 7)
    rows = jnp.stack([high, low, rest - low]).astype(bf16)
    return jnp.concatenate([state.astype(bf16), rows, jnp.zeros((13, HEAD_DIM), bf16)], axis=0)


def unpack(packed):
    decays = packed[:, HEAD_DIM : HEAD_DIM + 3].astype(f32).sum(axis=1)
    return (decays, packed[:, :HEAD_DIM])


def weights_before(decays, position):
    size = decays.shape[0]
    place = jnp.arange(size)
    earlier = place < position
    kept = jnp.where(earlier[:, None], decays, 0.0)
    after = (place[None, :] > place[:, None]).astype(f32)
    since = jnp.sum(after[:, :, None] * kept[None], axis=1)
    return (jnp.where(earlier[:, None], jnp.exp(since), 0.0), kept.sum(axis=0))


def weighted(weights, states):
    return jnp.sum(weights[:, None, :] * states.astype(f32), axis=0)


def body(
    tokens,
    norm_gain,
    w_filter_b,
    w_filter_c,
    w_filter_v,
    filter_taps,
    w_query,
    retention_gate_matrix,
    w_input,
    forget_gap,
    additive_fade_log,
    head_gain,
    initial_state,
    w_out_filter,
    w_out_rec,
):
    z, y, c = (lax.axis_index(a) for a in SP)
    own_rows = jnp.concatenate(
        [retention_gate_matrix, w_input, w_query, w_filter_b, w_filter_c, w_filter_v], axis=1
    )
    along_y = sent_to_all(own_rows, "sp_1").reshape(-1, own_rows.shape[1])
    weights = lax.all_gather(along_y, ("sp_0", "sp_2"), axis=0, tiled=True)
    gathered = sent_to_all(tokens, "tp").reshape(-1, tokens.shape[1])
    widened = gathered.astype(f32)
    normed = (
        widened
        * lax.rsqrt(jnp.mean(widened * widened, axis=-1, keepdims=True) + epsilon)
        * norm_gain
    ).astype(bf16)
    length, width = normed.shape
    order = np.arange(256).reshape(8, 2, 16).transpose(1, 0, 2).reshape(-1)
    swap = np.zeros((256, 256), np.float32)
    swap[order, np.arange(256)] = 1.0
    own = (
        jnp.einsum(
            "tzk,kl->tzl",
            normed.reshape(length, 8, 256),
            jnp.asarray(swap, bf16),
            preferred_element_type=f32,
        )
        .astype(bf16)
        .reshape(length, width)
    )
    partner = swapped(own, "sp_2")
    halo = shifted(own[length - HALO :], SP)
    fade = additive_fade_log
    head = lambda a, k: lax.dynamic_slice_in_dim(a, k * HEAD_DIM, HEAD_DIM, axis=1)
    partner_fade = swapped(head(fade, 1 - c), "sp_2")
    chip = jnp.concatenate([own, partner], axis=0)
    chip_gates = jnp.dot(chip, weights[:, :512], preferred_element_type=f32).astype(bf16)
    forget_logit, input_value = (chip_gates[:, :256], chip_gates[:, 256:])
    key_rate, log_decay = rates(forget_logit[:length], forget_gap, fade)
    value_in = silu(input_value[:length])
    gap_c = lax.dynamic_slice_in_dim(forget_gap, c * HEAD_DIM, HEAD_DIM)
    partner_rate, partner_decay = rates(head(forget_logit[length:], c), gap_c, partner_fade)
    partner_value = silu(head(input_value[length:], c))
    decay_own, state_own = state_of(head(key_rate, c), head(log_decay, c), head(value_in, c))
    decay_partner, state_partner = state_of(partner_rate, partner_decay, partner_value)
    first = c == 0
    decay_0, decay_1 = (
        jnp.where(first, decay_own, decay_partner),
        jnp.where(first, decay_partner, decay_own),
    )
    state_0, state_1 = (
        jnp.where(first, state_own, state_partner),
        jnp.where(first, state_partner, state_own),
    )
    state_chip = jnp.exp(decay_1)[None, :] * state_0 + state_1
    decays_y, states_y = unpack(sent_to_all(pack(decay_0 + decay_1, state_chip), "sp_1"))
    weights_row, decay_row = weights_before(decays_y, 8)
    row = weighted(weights_row, states_y)
    decays_z, states_z = unpack(sent_to_all(pack(decay_row, row), "sp_0"))
    weights_y, decay_y = weights_before(decays_y, y)
    inside = weighted(weights_y, states_y)
    weights_z, decay_z = weights_before(decays_z, z)
    start = lax.dynamic_index_in_dim(initial_state, c, keepdims=False).T
    before = jnp.exp(decay_z)[None, :] * start + weighted(weights_z, states_z)
    into_chip = jnp.exp(decay_y)[None, :] * before + inside
    into_second = jnp.exp(decay_0)[None, :] * into_chip + state_0
    incoming = exchanged(jnp.stack([into_chip, into_second]).astype(bf16), "sp_2")
    rest = jnp.dot(
        jnp.concatenate([halo, own], axis=0), weights[:, 512:], preferred_element_type=f32
    ).astype(bf16)
    queries = rest[HALO:, :256].astype(f32)
    gate_out = rest[HALO:, 256:512].astype(f32)
    product = rest[:, 512:768].astype(f32) * rest[:, 768:].astype(f32)
    filtered = jnp.zeros_like(gate_out)
    for offset in range(TAPS):
        at = HALO - (TAPS - 1) + offset
        filtered = filtered + filter_taps[offset] * product[at : at + length]
    filter_out = (gate_out * filtered).astype(bf16)
    filter_part = jnp.dot(filter_out, w_out_filter, preferred_element_type=f32)
    heads = lambda a: a.reshape(length // SPAN, SPAN, 2, HEAD_DIM)
    running = running_sum(log_decay)
    at_start = jnp.concatenate([jnp.zeros((1, 256), f32), running[SPAN - 1 : length - 1 : SPAN]])
    at_end = running[SPAN - 1 :: SPAN]
    within = running.reshape(length // SPAN, SPAN, 256) - at_start[:, None]
    scaled_query = heads((queries.reshape(within.shape) * jnp.exp(within)).astype(bf16))
    scaled_key = heads((key_rate.reshape(within.shape) * jnp.exp(-within)).astype(bf16))
    remainder = heads(
        (
            key_rate.reshape(within.shape)
            * jnp.exp(at_end[:, None] - running.reshape(within.shape))
        ).astype(bf16)
    )
    values = heads(value_in.astype(bf16))
    causal = jnp.tril(jnp.ones((SPAN, SPAN), dtype=bool))
    scores = jnp.einsum("bthk,bshk->bhts", scaled_query, scaled_key, preferred_element_type=f32)
    scores = jnp.where(causal, scores, 0.0).astype(bf16)
    local = jnp.einsum("bhts,bshv->bthv", scores, values, preferred_element_type=f32)
    cross = jnp.einsum("thk,shk->hts", scaled_query[1], remainder[0], preferred_element_type=f32)
    cross = jnp.einsum("hts,shv->thv", cross.astype(bf16), values[0], preferred_element_type=f32)
    local = jnp.concatenate([local[0], local[1] + cross], axis=0)
    full_query = (queries * jnp.exp(running)).astype(bf16).reshape(length, 2, HEAD_DIM)
    raw = local + jnp.einsum("thk,hvk->thv", full_query, incoming, preferred_element_type=f32)
    rec_out = (
        (raw * lax.rsqrt(jnp.mean(raw * raw, axis=-1, keepdims=True) + epsilon) * head_gain)
        .astype(bf16)
        .reshape(length, -1)
    )
    partial = (filter_part + jnp.dot(rec_out, w_out_rec, preferred_element_type=f32)).astype(bf16)
    arrived = exchanged(partial.reshape(4, length // 4, -1), "tp")
    return arrived.astype(f32).sum(axis=0).astype(bf16)


def solution(mesh):
    torus = Mesh(mesh.devices.reshape(8, 8, 2, mesh.shape["tp"]), ("sp_0", "sp_1", "sp_2", "tp"))
    placed = (
        P(SP_TP, None),
        P(),
        P(SP, "tp"),
        P(SP, "tp"),
        P(SP, "tp"),
        P(None, "tp"),
        P(SP, "tp"),
        P(SP, "tp"),
        P(SP, "tp"),
        P("tp"),
        P(SP, "tp"),
        P(),
        P("tp", None, None),
        P("tp", None),
        P("tp", None),
    )
    return jax.shard_map(
        body, mesh=torus, in_specs=placed, out_specs=P(SP_TP, None), check_vma=False
    )
```

profile of v0, /device:TPU:1, one launch (start us, length us, event | category | flops | bytes accessed | tf_op | source)
XLA Modules:
  0.0 157.7 jit_solution(3976584171746836471)
XLA Ops:
  6.6 0.8 constant_dynamic-update-slice_fusion.5
  10.9 19.2 %all_to_all.30 = bf16[8,16,1536]{2,1,0:T(8,128)(2,1)} all-to-all(bf16[8,16,1536]{2,1,0:T(8,128)(2,1)S(1)} %broadcast_in_dim.102), channel_id=1, replica_groups=mesh['sp_0'=8,'sp_1'=8,'sp_2'=2,'tp'=4] {'sp_1'}, dimensions={0} | all-to-all | bytes 786432 | tf_op jit(solution)/shard_map/all_to_all | solution.py:20
  30.1 1.8 %broadcast_in_dim.101 = bf16[4,32,2048]{2,1,0:T(8,128)(2,1)} broadcast(bf16[32,2048]{1,0:T(8,128)(2,1)} %param.16), dimensions={1,2} | broadcast | bytes 655360 | tf_op jit(solution)/shard_map/broadcast_in_dim | solution.py:24
  31.9 6.0 %all-to-all-start = ((bf16[4,32,2048]{2,1,0:T(8,128)(2,1)}), bf16[4,32,2048]{2,1,0:T(8,128)(2,1)S(1)}, u32[]{:S(2)}, u32[]{:S(2)}) async-start(bf16[4,32,2048]{2,1,0:T(8,128)(2,1)} %broadcast_in_dim.101), calls=%async_computation | async-start | bytes 1048576 | tf_op jit(solution)/shard_map/all_to_all | solution.py:20
  37.8 4.4 %collective-permute-start.2 = (f32[128,128]{1,0:T(8,128)S(1)}, f32[128,128]{1,0:T(8,128)S(1)}, u32[]{:S(2)}, u32[]{:S(2)}) collective-permute-start(f32[128,128]{1,0:T(8,128)S(1)} %constant_dynamic-slice_fusion.1), channel_id=1, source_target_pairs={{0,4},{4,0},{1,5},{5,1},{2,6},{6,2},{3,7},{7,3},{8,12},{12,8},{9,1... | collective-permute-start | bytes 196616 | tf_op jit(solution)/shard_map/ppermute | solution.py:28
  42.5 2.3 %all-to-all-done = bf16[4,32,2048]{2,1,0:T(8,128)(2,1)S(1)} async-done(((bf16[4,32,2048]{2,1,0:T(8,128)(2,1)}), bf16[4,32,2048]{2,1,0:T(8,128)(2,1)S(1)}, u32[]{:S(2)}, u32[]{:S(2)}) %all-to-all-start) | async-done | bytes 524320 | tf_op jit(solution)/shard_map/all_to_all | solution.py:20
  46.0 5.4 %collective-permute-start.1 = (bf16[128,2048]{0,1:T(8,128)(2,1)S(1)}, bf16[128,2048]{0,1:T(8,128)(2,1)}, u32[]{:S(2)}, u32[]{:S(2)}) collective-permute-start(bf16[128,2048]{0,1:T(8,128)(2,1)S(1)} %bitcast.98), channel_id=1, source_target_pairs={{0,4},{4,0},{1,5},{5,1},{2,6},{6,2},{3,7},{7,3},{8,12},{12,8},{9,1... | collective-permute-start | bytes 1572872 | tf_op jit(solution)/shard_map/ppermute | solution.py:28
  51.5 2.2 %collective-permute-start = (bf16[16,2048]{1,0:T(8,128)(2,1)S(1)}, bf16[16,2048]{1,0:T(8,128)(2,1)S(1)}, u32[]{:S(2)}, u32[]{:S(2)}) collective-permute-start(bf16[16,2048]{1,0:T(8,128)(2,1)S(1)} %bitcast.102), channel_id=1, source_target_pairs={{0,4},{4,8},{8,12},{12,16},{16,20},{20,24},{24,28},{28,32},{32,36}... | collective-permute-start | bytes 196616 | tf_op jit(solution)/shard_map/ppermute | solution.py:33
  53.6 1.3 collective-permute-done
  55.2 28.0 %all-gather.2.cloned.1.call-done = bf16[2048,1536]{1,0:T(8,128)(2,1)} async-done(((bf16[128,1536]{1,0:T(8,128)(2,1)}), bf16[2048,1536]{1,0:T(8,128)(2,1)}) %all-gather.2.cloned.1.call-update) | async-done | bytes 6291472 | tf_op jit(solution)/shard_map/all_gather | solution.py:106
  83.3 2.6 %fusion.8 = bf16[256,512]{1,0:T(8,128)(2,1)S(1)} fusion(bf16[2048,1536]{1,0:T(8,128)(2,1)} %all-gather.2.cloned.1.call-done, bf16[128,2048]{0,1:T(8,128)(2,1)} %collective-permute-done.1, bf16[128,2048]{0,1:T(8,128)(2,1)S(1)} %bitcast.99), kind=kOutput, calls=%fused_computation.8 | convolution fusion | flops 539099136 | bytes 3407872 | tf_op jit(solution)/shard_map/dot_general | solution.py:134
  86.1 0.8 copy-done.9
  86.9 1.3 fusion.5
  89.8 0.8 add_convert_fusion.1
  91.5 6.0 %all-to-all-start.2 = ((bf16[8,144,128]{2,1,0:T(8,128)(2,1)}), bf16[8,144,128]{2,1,0:T(8,128)(2,1)S(1)}, u32[]{:S(2)}, u32[]{:S(2)}) async-start(bf16[8,144,128]{2,1,0:T(8,128)(2,1)} %broadcast_in_dim.107), calls=%async_computation.2 | async-start | bytes 589824 | tf_op jit(solution)/shard_map/all_to_all | solution.py:20
  98.2 12.3 %all-to-all-done.2 = bf16[8,144,128]{2,1,0:T(8,128)(2,1)S(1)} async-done(((bf16[8,144,128]{2,1,0:T(8,128)(2,1)}), bf16[8,144,128]{2,1,0:T(8,128)(2,1)S(1)}, u32[]{:S(2)}, u32[]{:S(2)}) %all-to-all-start.2) | async-done | bytes 294944 | tf_op jit(solution)/shard_map/all_to_all | solution.py:20
  112.4 3.9 %all-to-all-start.3 = ((bf16[8,144,128]{2,1,0:T(8,128)(2,1)}), bf16[8,144,128]{2,1,0:T(8,128)(2,1)S(1)}, u32[]{:S(2)}, u32[]{:S(2)}) async-start(bf16[8,144,128]{2,1,0:T(8,128)(2,1)} %broadcast_in_dim.111), calls=%async_computation.3 | async-start | bytes 589824 | tf_op jit(solution)/shard_map/all_to_all | solution.py:20
  116.9 0.9 fusion.13
  118.1 9.4 %all-to-all-done.3 = bf16[8,144,128]{2,1,0:T(8,128)(2,1)S(1)} async-done(((bf16[8,144,128]{2,1,0:T(8,128)(2,1)}), bf16[8,144,128]{2,1,0:T(8,128)(2,1)S(1)}, u32[]{:S(2)}, u32[]{:S(2)}) %all-to-all-start.3) | async-done | bytes 294944 | tf_op jit(solution)/shard_map/all_to_all | solution.py:20
  127.9 0.9 convert_bitcast_fusion
  128.9 0.9 fusion.75
  129.8 5.5 %all_to_all.31 = bf16[2,128,128]{2,1,0:T(8,128)(2,1)S(1)} all-to-all(bf16[2,128,128]{2,1,0:T(8,128)(2,1)S(1)} %pad_maximum_fusion), channel_id=1, replica_groups=mesh['sp_0'=8,'sp_1'=8,'sp_2'=2,'tp'=4] {'sp_2'}, dimensions={0} | all-to-all | bytes 131072 | tf_op jit(solution)/shard_map/all_to_all | solution.py:20
  135.2 1.2 multiply_reduce_fusion.2
  137.7 12.4 %all_to_all.32 = bf16[4,32,2048]{2,1,0:T(8,128)(2,1)S(1)} all-to-all(bf16[4,32,2048]{2,1,0:T(8,128)(2,1)S(1)} %bitcast.94), channel_id=1, replica_groups=mesh['sp_0'=8,'sp_1'=8,'sp_2'=2,'tp'=4] {'tp'}, dimensions={0} | all-to-all | bytes 1048576 | tf_op jit(solution)/shard_map/all_to_all | solution.py:20
  (103 shorter events, 13.8 us)
Async XLA Ops:
  6.5 111.3 %copy-start = (bf16[256,2048]{1,0:T(8,128)(2,1)S(1)}, bf16[256,2048]{1,0:T(8,128)(2,1)}, u32[]{:S(2)}) copy-start(bf16[256,2048]{1,0:T(8,128)(2,1)} %param.29) | copy-start | bytes 3145732
  6.5 31.3 %copy-start.3 = (f32[128,256]{1,0:T(8,128)S(1)}, f32[128,256]{1,0:T(8,128)}, u32[]{:S(2)}) copy-start(f32[128,256]{1,0:T(8,128)} %param.26) | copy-start | bytes 393220
  6.5 35.7 %copy-start.5 = (f32[2,128,128]{2,1,0:T(8,128)S(1)}, f32[2,128,128]{2,1,0:T(8,128)}, u32[]{:S(2)}) copy-start(f32[2,128,128]{2,1,0:T(8,128)} %param.28) | copy-start | bytes 393220
  6.5 35.7 %copy-start.6 = (f32[2048]{0:T(1024)S(1)}, f32[2048]{0:T(1024)}, u32[]{:S(2)}) copy-start(f32[2048]{0:T(1024)} %param.17) | copy-start | bytes 24580
  6.5 35.9 %copy-start.8 = (f32[256]{0:T(256)S(1)}, f32[256]{0:T(256)}, u32[]{:S(2)}) copy-start(f32[256]{0:T(256)} %param.25) | copy-start | bytes 3076
  6.5 76.7 %all-gather.2.cloned.1.call-start = ((), (), s32[]{:S(2)}) async-start(), calls=%async_computation.6 | async-start | bytes 6684672 | tf_op jit(solution)/shard_map/all_gather | solution.py:106
  31.9 12.9 %all-to-all-start = ((bf16[4,32,2048]{2,1,0:T(8,128)(2,1)}), bf16[4,32,2048]{2,1,0:T(8,128)(2,1)S(1)}, u32[]{:S(2)}, u32[]{:S(2)}) async-start(bf16[4,32,2048]{2,1,0:T(8,128)(2,1)} %broadcast_in_dim.101), calls=%async_computation | async-start | bytes 1048576 | tf_op jit(solution)/shard_map/all_to_all | solution.py:20
  37.8 7.6 %copy-start.4 = (bf16[256,256,1]{1,0,2:T(8,128)(2,1)S(1)}, bf16[256,256,1]{1,0,2:T(8,128)(2,1)}, u32[]{:S(2)}) copy-start(bf16[256,256,1]{1,0,2:T(8,128)(2,1)} %constant.72) | copy-start | bytes 393220
  37.8 50.8 %collective-permute-start.2 = (f32[128,128]{1,0:T(8,128)S(1)}, f32[128,128]{1,0:T(8,128)S(1)}, u32[]{:S(2)}, u32[]{:S(2)}) collective-permute-start(f32[128,128]{1,0:T(8,128)S(1)} %constant_dynamic-slice_fusion.1), channel_id=1, source_target_pairs={{0,4},{4,0},{1,5},{5,1},{2,6},{6,2},{3,7},{7,3},{8,12},{12,8},{9,1... | collective-permute-start | bytes 196616 | tf_op jit(solution)/shard_map/ppermute | solution.py:28
  44.9 6.5 %copy-start.7 = (f32[3,256]{1,0:T(4,128)S(1)}, f32[3,256]{1,0:T(4,128)}, u32[]{:S(2)}) copy-start(f32[3,256]{1,0:T(4,128)} %param.21) | copy-start | bytes 9220
  46.0 9.2 %collective-permute-start.1 = (bf16[128,2048]{0,1:T(8,128)(2,1)S(1)}, bf16[128,2048]{0,1:T(8,128)(2,1)}, u32[]{:S(2)}, u32[]{:S(2)}) collective-permute-start(bf16[128,2048]{0,1:T(8,128)(2,1)S(1)} %bitcast.98), channel_id=1, source_target_pairs={{0,4},{4,0},{1,5},{5,1},{2,6},{6,2},{3,7},{7,3},{8,12},{12,8},{9,1... | collective-permute-start | bytes 1572872 | tf_op jit(solution)/shard_map/ppermute | solution.py:28
  51.5 3.5 %collective-permute-start = (bf16[16,2048]{1,0:T(8,128)(2,1)S(1)}, bf16[16,2048]{1,0:T(8,128)(2,1)S(1)}, u32[]{:S(2)}, u32[]{:S(2)}) collective-permute-start(bf16[16,2048]{1,0:T(8,128)(2,1)S(1)} %bitcast.102), channel_id=1, source_target_pairs={{0,4},{4,8},{8,12},{12,16},{16,20},{20,24},{24,28},{28,32},{32,36}... | collective-permute-start | bytes 196616 | tf_op jit(solution)/shard_map/ppermute | solution.py:33
  83.3 3.6 %copy-start.9 = (bf16[2048,1536]{1,0:T(8,128)(2,1)S(1)}, bf16[2048,1536]{1,0:T(8,128)(2,1)}, u32[]{:S(2)}) copy-start(bf16[2048,1536]{1,0:T(8,128)(2,1)} %all-gather.2.cloned.1.call-done) | copy-start | bytes 18874372
  88.1 29.7 %copy-start.2 = (bf16[144,1024]{1,0:T(8,128)(2,1)}, bf16[144,1024]{1,0:T(8,128)(2,1)S(1)}, u32[]{:S(2)}) copy-start(bf16[144,1024]{1,0:T(8,128)(2,1)S(1)} %fusion.5) | copy-start | bytes 884740
  91.5 18.9 %all-to-all-start.2 = ((bf16[8,144,128]{2,1,0:T(8,128)(2,1)}), bf16[8,144,128]{2,1,0:T(8,128)(2,1)S(1)}, u32[]{:S(2)}, u32[]{:S(2)}) async-start(bf16[8,144,128]{2,1,0:T(8,128)(2,1)} %broadcast_in_dim.107), calls=%async_computation.2 | async-start | bytes 589824 | tf_op jit(solution)/shard_map/all_to_all | solution.py:20
  112.4 15.2 %all-to-all-start.3 = ((bf16[8,144,128]{2,1,0:T(8,128)(2,1)}), bf16[8,144,128]{2,1,0:T(8,128)(2,1)S(1)}, u32[]{:S(2)}, u32[]{:S(2)}) async-start(bf16[8,144,128]{2,1,0:T(8,128)(2,1)} %broadcast_in_dim.111), calls=%async_computation.3 | async-start | bytes 589824 | tf_op jit(solution)/shard_map/all_to_all | solution.py:20
  127.9 9.4 %copy-start.1 = (bf16[256,2048]{1,0:T(8,128)(2,1)S(1)}, bf16[256,2048]{1,0:T(8,128)(2,1)}, u32[]{:S(2)}) copy-start(bf16[256,2048]{1,0:T(8,128)(2,1)} %param.30) | copy-start | bytes 3145732
Sparse Core Ops, SparseCore 0:
  30.2 53.0 all-gather.1
where the time goes:
time: 159 us; the launch traced here: 158 us
  waiting for transfers between devices  53.3 us (34%)
  blocking collectives  37 us (23%)
  starting transfers between devices  27.8 us (17%)
  between operations  13.9 us (9%)
  local copies, waits for them, and re-layouts  10.7 us (7%)
  matrix products  8.98 us (6%)
  other arithmetic  5.94 us (4%)
    all_to_all x3, blocking collectives, exchanged(): return lax.all_to_all(blocks, axis, split_axis=0, concat_axis=0, tiled=True)  37 us
    all_gather x1, waiting for transfers between devices, body(): weights = lax.all_gather(along_y, ('sp_0', 'sp_2'), axis=0, tiled=True)  28 us
    all_to_all x3, waiting for transfers between devices, exchanged(): return lax.all_to_all(blocks, axis, split_axis=0, concat_axis=0, tiled=True)  24 us
    all_to_all x3, starting transfers between devices, exchanged(): return lax.all_to_all(blocks, axis, split_axis=0, concat_axis=0, tiled=True)  15.8 us
    ppermute x2, starting transfers between devices, swapped(): return lax.ppermute(x, axis, [(0, 1), (1, 0)])  9.76 us
    unnamed x27, local copies, waits for them, and re-layouts  4.51 us
    broadcast_in_dim x4, local copies, waits for them, and re-layouts, sent_to_all(): return exchanged(jnp.broadcast_to(x, (lax.axis_size(axis), *x.shape)), axis)  3.29 us
  transfers between devices with their start and end apart: 7, of which 5 were waited for; matrix products, arithmetic and copies ran while one was open for 7% of the time, Pallas kernels for 0%

commit v1 on v0

--- a/solution.py
+++ b/solution.py
@@ -103,7 +103,15 @@
         [retention_gate_matrix, w_input, w_query, w_filter_b, w_filter_c, w_filter_v], axis=1
     )
     along_y = sent_to_all(own_rows, "sp_1").reshape(-1, own_rows.shape[1])
-    weights = lax.all_gather(along_y, ("sp_0", "sp_2"), axis=0, tiled=True)
+    weights = jnp.concatenate(
+        lax.all_to_all(
+            jnp.stack([along_y for _ in range(lax.psum(1, axis_name=("sp_0", "sp_2")))]),
+            axis_name=("sp_0", "sp_2"),
+            concat_axis=0,
+            split_axis=0,
+        ),
+        axis=0,
+    )
     gathered = sent_to_all(tokens, "tp").reshape(-1, tokens.shape[1])
     widened = gathered.astype(f32)
     normed = (

time: 159 us -> 254 us (1.60)
  waiting for transfers between devices: 53.3 us -> 154 us
  between operations: 13.9 us -> 0.55 us
  starting transfers between devices: 27.8 us -> 36.8 us
  other arithmetic: 5.94 us -> 2.32 us
    all_to_all x0 -> x1, waiting for transfers between devices: none -> 128 us  [body(): lax.all_to_all(jnp.stack([along_y for _ in range(lax.psum(1, axis_name=('...]
    all_gather x1 -> x0, waiting for transfers between devices: 28 us -> none  [body(): weights = lax.all_gather(along_y, ('sp_0', 'sp_2'), axis=0, tiled=True)]
    all_to_all x0 -> x1, starting transfers between devices: none -> 14.5 us  [body(): lax.all_to_all(jnp.stack([along_y for _ in range(lax.psum(1, axis_name=('...]
    ppermute x2, starting transfers between devices: 9.76 us -> 4.46 us  [swapped(): return lax.ppermute(x, axis, [(0, 1), (1, 0)])]
    another operation x1 -> x2, local copies, waits for them, and re-layouts: 0.01 us -> 3.27 us  [the longest x1 3.26 us: body(): jnp.stack([along_y for _ in range(lax.psum(1, axis_name=('sp_0', 'sp_2')))])]
  transfers between devices with their start and end apart: 7 -> 7, of which waited for: 5 -> 5; matrix products, arithmetic and copies ran while one was open for 7% -> 5% of each run, Pallas kernels for 0% -> 0%
where the time goes in v1:
time: 254 us; the launch traced here: 253 us
  waiting for transfers between devices  154 us (61%)
  starting transfers between devices  36.8 us (14%)
  blocking collectives  36.5 us (14%)
  local copies, waits for them, and re-layouts  12.6 us (5%)
  matrix products  10.1 us (4%)
    all_to_all x1, waiting for transfers between devices, body(): lax.all_to_all(jnp.stack([along_y for _ in range(lax.psum(1, axis_name=('...  128 us
    all_to_all x3, blocking collectives, exchanged(): return lax.all_to_all(blocks, axis, split_axis=0, concat_axis=0, tiled=True)  36.5 us
    all_to_all x3, waiting for transfers between devices, exchanged(): return lax.all_to_all(blocks, axis, split_axis=0, concat_axis=0, tiled=True)  24.4 us
    all_to_all x3, starting transfers between devices, exchanged(): return lax.all_to_all(blocks, axis, split_axis=0, concat_axis=0, tiled=True)  15.6 us
    all_to_all x1, starting transfers between devices, body(): lax.all_to_all(jnp.stack([along_y for _ in range(lax.psum(1, axis_name=('...  14.5 us
  transfers between devices with their start and end apart: 7, of which 5 were waited for; matrix products, arithmetic and copies ran while one was open for 5% of the time, Pallas kernels for 0%

profile of v1, /device:TPU:1, one launch (start us, length us, event | category | flops | bytes accessed | tf_op | source)
XLA Modules:
  0.0 252.9 jit_solution(19449111124146691)
XLA Ops:
  0.0 1.8 broadcast_in_dim.101
  1.8 4.8 %all-to-all-start = ((bf16[4,32,2048]{2,1,0:T(8,128)(2,1)}), bf16[4,32,2048]{2,1,0:T(8,128)(2,1)S(1)}, u32[]{:S(2)}, u32[]{:S(2)}) async-start(bf16[4,32,2048]{2,1,0:T(8,128)(2,1)} %broadcast_in_dim.101), calls=%async_computation | async-start | bytes 1048576 | tf_op jit(solution)/shard_map/all_to_all | solution.py:20
  8.1 0.7 constant_dynamic-update-slice_fusion.3
  10.9 2.7 %all-to-all-done = bf16[4,32,2048]{2,1,0:T(8,128)(2,1)S(1)} async-done(((bf16[4,32,2048]{2,1,0:T(8,128)(2,1)}), bf16[4,32,2048]{2,1,0:T(8,128)(2,1)S(1)}, u32[]{:S(2)}, u32[]{:S(2)}) %all-to-all-start) | async-done | bytes 524320 | tf_op jit(solution)/shard_map/all_to_all | solution.py:20
  13.6 19.6 %all_to_all.35 = bf16[8,16,1536]{2,1,0:T(8,128)(2,1)S(1)} all-to-all(bf16[8,16,1536]{2,1,0:T(8,128)(2,1)S(1)} %broadcast_in_dim.102), channel_id=1, replica_groups=mesh['sp_0'=8,'sp_1'=8,'sp_2'=2,'tp'=4] {'sp_1'}, dimensions={0} | all-to-all | bytes 786432 | tf_op jit(solution)/shard_map/all_to_all | solution.py:20
  33.2 3.3 %stack.25 = bf16[16,128,1536]{2,1,0:T(8,128)(2,1)} broadcast(bf16[128,1536]{1,0:T(8,128)(2,1)S(1)} %bitcast.96), dimensions={1,2} | broadcast | bytes 6684672 | tf_op jit(solution)/shard_map/stack | solution.py:108
  36.5 14.5 %all-to-all-start.2 = ((bf16[16,128,1536]{2,1,0:T(8,128)(2,1)}), bf16[16,128,1536]{2,1,0:T(8,128)(2,1)}, u32[]{:S(2)}, u32[]{:S(2)}) async-start(bf16[16,128,1536]{2,1,0:T(8,128)(2,1)} %stack.25), calls=%async_computation.2 | async-start | bytes 12582912 | tf_op jit(solution)/shard_map/all_to_all | solution.py:107
  51.1 2.2 collective-permute-start.2
  54.8 2.3 collective-permute-start.1
  57.1 2.2 collective-permute-start
  59.4 1.3 collective-permute-done
  61.0 128.4 %all-to-all-done.2 = bf16[16,128,1536]{2,1,0:T(8,128)(2,1)} async-done(((bf16[16,128,1536]{2,1,0:T(8,128)(2,1)}), bf16[16,128,1536]{2,1,0:T(8,128)(2,1)}, u32[]{:S(2)}, u32[]{:S(2)}) %all-to-all-start.2) | async-done | bytes 6291488 | tf_op jit(solution)/shard_map/all_to_all | solution.py:107
  189.4 2.5 fusion.8
  192.1 3.5 %fusion.5 = bf16[144,1024]{1,0:T(8,128)(2,1)S(1)} fusion(bf16[2048,1536]{1,0:T(8,128)(2,1)} %bitcast.3, bf16[128,2048]{0,1:T(8,128)(2,1)S(1)} %bitcast.101, bf16[16,2048]{0,1:T(8,128)(2,1)S(1)} %copy.85), kind=kOutput, calls=%fused_computation.7 | convolution fusion | flops 605306880 | bytes 5079040 | tf_op jit(solution)/shard_map/dot_general | solution.py:173
  197.0 0.7 broadcast_in_dim.107
  197.8 3.6 %all-to-all-start.3 = ((bf16[8,144,128]{2,1,0:T(8,128)(2,1)}), bf16[8,144,128]{2,1,0:T(8,128)(2,1)S(1)}, u32[]{:S(2)}, u32[]{:S(2)}) async-start(bf16[8,144,128]{2,1,0:T(8,128)(2,1)} %broadcast_in_dim.107), calls=%async_computation.3 | async-start | bytes 589824 | tf_op jit(solution)/shard_map/all_to_all | solution.py:20
  202.0 10.5 %all-to-all-done.3 = bf16[8,144,128]{2,1,0:T(8,128)(2,1)S(1)} async-done(((bf16[8,144,128]{2,1,0:T(8,128)(2,1)}), bf16[8,144,128]{2,1,0:T(8,128)(2,1)S(1)}, u32[]{:S(2)}, u32[]{:S(2)}) %all-to-all-start.3) | async-done | bytes 294944 | tf_op jit(solution)/shard_map/all_to_all | solution.py:20
  213.1 0.7 broadcast_in_dim.111
  213.8 7.3 %all-to-all-start.4 = ((bf16[8,144,128]{2,1,0:T(8,128)(2,1)}), bf16[8,144,128]{2,1,0:T(8,128)(2,1)S(1)}, u32[]{:S(2)}, u32[]{:S(2)}) async-start(bf16[8,144,128]{2,1,0:T(8,128)(2,1)} %broadcast_in_dim.111), calls=%async_computation.4 | async-start | bytes 589824 | tf_op jit(solution)/shard_map/all_to_all | solution.py:20
  221.7 11.1 %all-to-all-done.4 = bf16[8,144,128]{2,1,0:T(8,128)(2,1)S(1)} async-done(((bf16[8,144,128]{2,1,0:T(8,128)(2,1)}), bf16[8,144,128]{2,1,0:T(8,128)(2,1)S(1)}, u32[]{:S(2)}, u32[]{:S(2)}) %all-to-all-start.4) | async-done | bytes 294944 | tf_op jit(solution)/shard_map/all_to_all | solution.py:20
  233.3 5.2 %all_to_all.36 = bf16[2,128,128]{2,1,0:T(8,128)(2,1)S(1)} all-to-all(bf16[2,128,128]{2,1,0:T(8,128)(2,1)S(1)} %pad_maximum_fusion), channel_id=1, replica_groups=mesh['sp_0'=8,'sp_1'=8,'sp_2'=2,'tp'=4] {'sp_2'}, dimensions={0} | all-to-all | bytes 131072 | tf_op jit(solution)/shard_map/all_to_all | solution.py:20
  239.0 1.6 fusion.2
  240.6 11.6 %all_to_all.37 = bf16[4,32,2048]{2,1,0:T(8,128)(2,1)S(1)} all-to-all(bf16[4,32,2048]{2,1,0:T(8,128)(2,1)S(1)} %bitcast.95), channel_id=1, replica_groups=mesh['sp_0'=8,'sp_1'=8,'sp_2'=2,'tp'=4] {'tp'}, dimensions={0} | all-to-all | bytes 1048576 | tf_op jit(solution)/shard_map/all_to_all | solution.py:20
  252.2 0.7 reduce_sum.145
  (99 shorter events, 9.5 us)
Async XLA Ops:
  0.0 221.4 %copy-start = (bf16[256,2048]{1,0:T(8,128)(2,1)S(1)}, bf16[256,2048]{1,0:T(8,128)(2,1)}, u32[]{:S(2)}) copy-start(bf16[256,2048]{1,0:T(8,128)(2,1)} %param.29) | copy-start | bytes 3145732
  1.8 11.8 %all-to-all-start = ((bf16[4,32,2048]{2,1,0:T(8,128)(2,1)}), bf16[4,32,2048]{2,1,0:T(8,128)(2,1)S(1)}, u32[]{:S(2)}, u32[]{:S(2)}) async-start(bf16[4,32,2048]{2,1,0:T(8,128)(2,1)} %broadcast_in_dim.101), calls=%async_computation | async-start | bytes 1048576 | tf_op jit(solution)/shard_map/all_to_all | solution.py:20
  36.5 14.6 %copy-start.1 = (f32[128,256]{1,0:T(8,128)S(1)}, f32[128,256]{1,0:T(8,128)}, u32[]{:S(2)}) copy-start(f32[128,256]{1,0:T(8,128)} %param.26) | copy-start | bytes 393220
  36.5 16.8 %copy-start.4 = (f32[2048]{0:T(1024)S(1)}, f32[2048]{0:T(1024)}, u32[]{:S(2)}) copy-start(f32[2048]{0:T(1024)} %param.17) | copy-start | bytes 24580
  36.5 16.8 %copy-start.3 = (f32[2,128,128]{2,1,0:T(8,128)S(1)}, f32[2,128,128]{2,1,0:T(8,128)}, u32[]{:S(2)}) copy-start(f32[2,128,128]{2,1,0:T(8,128)} %param.28) | copy-start | bytes 393220
  36.5 16.9 %copy-start.6 = (f32[256]{0:T(256)S(1)}, f32[256]{0:T(256)}, u32[]{:S(2)}) copy-start(f32[256]{0:T(256)} %param.25) | copy-start | bytes 3076
  36.5 152.9 %all-to-all-start.2 = ((bf16[16,128,1536]{2,1,0:T(8,128)(2,1)}), bf16[16,128,1536]{2,1,0:T(8,128)(2,1)}, u32[]{:S(2)}, u32[]{:S(2)}) async-start(bf16[16,128,1536]{2,1,0:T(8,128)(2,1)} %stack.25), calls=%async_computation.2 | async-start | bytes 12582912 | tf_op jit(solution)/shard_map/all_to_all | solution.py:107
  51.0 3.2 %copy-start.2 = (bf16[256,256,1]{1,0,2:T(8,128)(2,1)S(1)}, bf16[256,256,1]{1,0,2:T(8,128)(2,1)}, u32[]{:S(2)}) copy-start(bf16[256,256,1]{1,0,2:T(8,128)(2,1)} %constant.72) | copy-start | bytes 393220
  51.0 6.0 %copy-start.5 = (f32[3,256]{1,0:T(4,128)S(1)}, f32[3,256]{1,0:T(4,128)}, u32[]{:S(2)}) copy-start(f32[3,256]{1,0:T(4,128)} %param.21) | copy-start | bytes 9220
  51.1 145.0 %collective-permute-start.2 = (f32[128,128]{1,0:T(8,128)S(1)}, f32[128,128]{1,0:T(8,128)S(1)}, u32[]{:S(2)}, u32[]{:S(2)}) collective-permute-start(f32[128,128]{1,0:T(8,128)S(1)} %constant_dynamic-slice_fusion.1), channel_id=1, source_target_pairs={{0,4},{4,0},{1,5},{5,1},{2,6},{6,2},{3,7},{7,3},{8,12},{12,8},{9,1... | collective-permute-start | bytes 196616 | tf_op jit(solution)/shard_map/ppermute | solution.py:28
  54.8 6.2 %collective-permute-start.1 = (bf16[128,2048]{0,1:T(8,128)(2,1)S(1)}, bf16[128,2048]{0,1:T(8,128)(2,1)}, u32[]{:S(2)}, u32[]{:S(2)}) collective-permute-start(bf16[128,2048]{0,1:T(8,128)(2,1)S(1)} %bitcast.99), channel_id=1, source_target_pairs={{0,4},{4,0},{1,5},{5,1},{2,6},{6,2},{3,7},{7,3},{8,12},{12,8},{9,1... | collective-permute-start | bytes 1572872 | tf_op jit(solution)/shard_map/ppermute | solution.py:28
  57.1 3.5 %collective-permute-start = (bf16[16,2048]{1,0:T(8,128)(2,1)S(1)}, bf16[16,2048]{1,0:T(8,128)(2,1)S(1)}, u32[]{:S(2)}, u32[]{:S(2)}) collective-permute-start(bf16[16,2048]{1,0:T(8,128)(2,1)S(1)} %bitcast.103), channel_id=1, source_target_pairs={{0,4},{4,8},{8,12},{12,16},{16,20},{20,24},{24,28},{28,32},{32,36}... | collective-permute-start | bytes 196616 | tf_op jit(solution)/shard_map/ppermute | solution.py:33
  197.8 41.0 %copy-start.7 = (f32[128]{0:T(128)S(1)}, f32[128]{0:T(128)}, u32[]{:S(2)}) copy-start(f32[128]{0:T(128)} %param.27) | copy-start | bytes 1540
  197.8 14.7 %all-to-all-start.3 = ((bf16[8,144,128]{2,1,0:T(8,128)(2,1)}), bf16[8,144,128]{2,1,0:T(8,128)(2,1)S(1)}, u32[]{:S(2)}, u32[]{:S(2)}) async-start(bf16[8,144,128]{2,1,0:T(8,128)(2,1)} %broadcast_in_dim.107), calls=%async_computation.3 | async-start | bytes 589824 | tf_op jit(solution)/shard_map/all_to_all | solution.py:20
  213.8 19.0 %all-to-all-start.4 = ((bf16[8,144,128]{2,1,0:T(8,128)(2,1)}), bf16[8,144,128]{2,1,0:T(8,128)(2,1)S(1)}, u32[]{:S(2)}, u32[]{:S(2)}) async-start(bf16[8,144,128]{2,1,0:T(8,128)(2,1)} %broadcast_in_dim.111), calls=%async_computation.4 | async-start | bytes 589824 | tf_op jit(solution)/shard_map/all_to_all | solution.py:20
